TPU v7x, 128 devices: a whole 4x4x4 slice. The times are simulated.
128 devices in a mesh: sp: 64 (over z, y, x), tp: 2 (over core).
Axes of the slice: x: 4, y: 4, z: 4, core: 2. Of those that a mesh axis runs over, the one named last changes fastest.
Arguments:
- mid_rows: bfloat16 [16384, 2048], P(('sp', 'tp')), may hold values from -6 to 6
- cotangent: bfloat16 [16384, 2048], P(('sp', 'tp')), may hold values from -24 to 24
- routes: int32 [16384, 2], P(('sp', 'tp')), may hold values from 0 to 63, all different within a row; in each aligned block of 128 rows (0 to 127, 128 to 255, ...) at most 8 rows name the same one
- route_weight: float32 [16384, 2], P(('sp', 'tp')), may hold values from 0.3 to 2
- filtered: bfloat16 [16384, 2048], P('sp', 'tp'), may hold values from -30 to 30
- conv_taps: float32 [31, 2048], P(None, 'tp'), may hold values from -1 to 1
- norm_gain: float32 [2048], P('tp'), may hold values from 0.1 to 1.9
- out_weight: bfloat16 [2048, 2048], P('tp'), may hold values from -0.125 to 0.125
- gate_weight: bfloat16 [64, 2048, 1024], P('sp', None, 'tp'), may hold values from -0.125 to 0.125
- up_weight: bfloat16 [64, 2048, 1024], P('sp', None, 'tp'), may hold values from -0.125 to 0.125
- down_weight: bfloat16 [64, 1024, 2048], P('sp', 'tp'), may hold values from -0.1875 to 0.1875
Outputs:
- gate_grad: float32 [64, 2048, 1024], P('sp', None, 'tp')
- up_grad: float32 [64, 2048, 1024], P('sp', None, 'tp')
- down_grad: float32 [64, 1024, 2048], P('sp', 'tp')
- proj_grad: float32 [2048, 2048], P('sp', 'tp')
- input_grad: bfloat16 [16384, 2048], P('sp', 'tp')
Inputs may be any that keep to these rules, and one draw needn't show every extreme that they name: `routes`: each row names 2 different experts. In each aligned block of 128 rows no expert is named by more than 8 rows.
All inputs are finite; a program needn't handle non-finite values.
Results may differ from a plain program's by a relative error of at most 0.0075.
Values may be sent and summed in bfloat16 or wider, within the bound.
A program may use at most 128 MiB of HBM per device.

v0:
```python
import jax
import jax.numpy as jnp
from jax import lax
from jax.sharding import Mesh
from jax.sharding import PartitionSpec as P

SP = ("sp_0", "sp_1", "sp_2")
SP_TP = ("sp_0", "sp_1", "sp_2", "tp")


NORM_EPS = 1e-05


def total_of_pieces(value, axis):
    return lax.all_gather(value, axis).sum(0)


def sent_together(arrays, axis, split_dim, concat_dim, along):
    widths = [a.shape[along] for a in arrays]
    both = jnp.concatenate(arrays, axis=along)
    whole = lax.all_to_all(both, axis, split_axis=split_dim, concat_axis=concat_dim, tiled=True)
    return tuple(jnp.split(whole, [sum(widths[:k]) for k in range(1, len(widths))], axis=along))


def sent_together_2(arrays, axis, dim, along):
    both = jnp.concatenate(arrays, axis=along)
    whole, at, finished = (lax.all_gather(both, axis, axis=dim, tiled=True), 0, [])
    for a in arrays:
        finished.append(lax.slice_in_dim(whole, at, at + a.shape[along], axis=along))
        at += a.shape[along]
    return tuple(finished)


def cut_along(value, dim, peers):
    before, after = (value.shape[:dim], value.shape[dim + 1 :])
    return jnp.moveaxis(value.reshape(*before, peers, -1, *after), dim, 0)


def sent_and_summed(value, axis, dim):
    pieces = cut_along(value, dim, lax.axis_size(axis))
    arrived = lax.all_to_all(pieces, axis, split_axis=0, concat_axis=0, tiled=True)
    return arrived.astype(jnp.float32).sum(axis=0)


def in_order(pieces, dim):
    pieces = jnp.moveaxis(pieces, 0, dim)
    dims = pieces.shape
    return pieces.reshape(*dims[:dim], dims[dim] * dims[dim + 1], *dims[dim + 2 :])


def copy_for_each(value, axis):
    copies = jnp.broadcast_to(value, (lax.axis_size(axis), *value.shape))
    return lax.all_to_all(copies, axis, split_axis=0, concat_axis=0, tiled=True)


def collect(value, axis, dim):
    return in_order(copy_for_each(value, axis), dim)


def sum_by_axis(so_far, axes):
    for axis in axes:
        so_far = lax.psum_scatter(so_far, axis, scatter_dimension=0, tiled=True)
    return so_far


def extended(block, sides, width):
    for axis, dim in sides:
        count = lax.axis_size(axis)
        forward = [(i, i + 1) for i in range(count - 1)]
        backward = [(target, source) for source, target in forward]
        low = lax.ppermute(
            lax.slice_in_dim(block, block.shape[dim] - width, None, axis=dim), axis, forward
        )
        high = lax.ppermute(lax.slice_in_dim(block, 0, width, axis=dim), axis, backward)
        block = jnp.concatenate([low, block, high], axis=dim)
    return block


def silu_grad(pre_act):
    logistic = jax.nn.sigmoid(pre_act)
    return logistic * (1.0 + pre_act * (1.0 - logistic))


def assign_slots(routes, experts, capacity):
    token_count, per_token = routes.shape
    flattened = routes.reshape(token_count * per_token)
    one_hot = (flattened[:, None] == jnp.arange(experts, dtype=jnp.int32)[None, :]).astype(
        jnp.int32
    )
    earlier = jnp.cumsum(one_hot, axis=0) - one_hot
    positions = jnp.sum(earlier * one_hot, axis=1)
    target = flattened * capacity + positions
    route_ids = jnp.arange(token_count * per_token, dtype=jnp.int32)
    slot_owner = (
        jnp.full((experts * capacity,), token_count * per_token, jnp.int32)
        .at[target]
        .set(route_ids)
    )
    return (slot_owner, target)


def expert_backward(inputs, routed, gate_mat, up_mat, down_mat):
    pre_gate = jnp.einsum("secd,edf->secf", inputs, gate_mat, preferred_element_type=jnp.float32)
    pre_up = jnp.einsum("secd,edf->secf", inputs, up_mat, preferred_element_type=jnp.float32)
    gate_act = jax.nn.silu(pre_gate)
    hidden = (gate_act * pre_up).astype(jnp.bfloat16)
    down_part = jnp.einsum("secf,secd->efd", hidden, routed, preferred_element_type=jnp.float32)
    hidden_grad = jnp.einsum("secd,efd->secf", routed, down_mat, preferred_element_type=jnp.float32)
    gate_pre = (hidden_grad * pre_up * silu_grad(pre_gate)).astype(jnp.bfloat16)
    up_pre = (hidden_grad * gate_act).astype(jnp.bfloat16)
    gate_part = jnp.einsum("secd,secf->edf", inputs, gate_pre, preferred_element_type=jnp.float32)
    up_part = jnp.einsum("secd,secf->edf", inputs, up_pre, preferred_element_type=jnp.float32)
    return (gate_pre, up_pre, gate_part, up_part, down_part)


def input_part(gate_pre, up_pre, gate_mat, up_mat):
    first_term = jnp.einsum(
        "secf,edf->secd", gate_pre, gate_mat, preferred_element_type=jnp.float32
    )
    return first_term + jnp.einsum(
        "secf,edf->secd", up_pre, up_mat, preferred_element_type=jnp.float32
    )


def per_device(
    mid_rows,
    cotangent,
    routes,
    route_weight,
    filtered,
    conv_taps,
    norm_gain,
    out_weight,
    gate_weight,
    up_weight,
    down_weight,
):
    sp_count = lax.axis_size(SP)
    token_count, model_width = mid_rows.shape
    per_token = routes.shape[1]
    local_experts = gate_weight.shape[0]
    experts = local_experts * sp_count
    capacity = 2 * token_count * per_token // sp_count
    values = filtered.astype(jnp.float32)
    channel_sum, squares = (
        total_of_pieces(jnp.sum(values, axis=1), "tp"),
        total_of_pieces(jnp.sum(values * values, axis=1), "tp"),
    )
    slot_owner, target = assign_slots(routes, experts, capacity)
    token_of = slot_owner // per_token
    inputs = jnp.take(mid_rows, token_of, axis=0, mode="fill", fill_value=0)
    route_scale = jnp.take(
        route_weight.reshape(token_count * per_token), slot_owner, mode="fill", fill_value=0.0
    )
    cot_rows = jnp.take(cotangent, token_of, axis=0, mode="fill", fill_value=0)
    routed = (route_scale[:, None] * cot_rows.astype(jnp.float32)).astype(jnp.bfloat16)
    inputs = inputs.reshape(sp_count, local_experts, capacity, model_width)
    routed = routed.reshape(sp_count, local_experts, capacity, model_width)
    got_in, got_cot = sent_together((inputs, routed), SP, 0, 0, 1)
    all_in, all_cot = sent_together_2((got_in, got_cot), "tp", 0, 1)
    gate_pre, up_pre, gate_part, up_part, down_part = expert_backward(
        all_in, all_cot, gate_weight, up_weight, down_weight
    )
    partial_rows = input_part(gate_pre, up_pre, gate_weight, up_weight).astype(jnp.bfloat16)
    back_rows = sent_and_summed(partial_rows, "tp", 0).astype(jnp.bfloat16)
    returned = lax.all_to_all(back_rows, SP, split_axis=0, concat_axis=0, tiled=True)
    gate_grad, up_grad, down_grad = (gate_part, up_part, down_part)
    back_all = returned.reshape(experts * capacity, model_width)
    route_rows = jnp.take(back_all, target, axis=0)
    route_sum = jnp.sum(
        route_rows.astype(jnp.float32).reshape(token_count, per_token, model_width), axis=1
    )
    mid_grad = (cotangent.astype(jnp.float32) + route_sum).astype(jnp.bfloat16)
    average = channel_sum / model_width
    variance = squares / model_width - average * average
    inv_scale = lax.rsqrt(variance + NORM_EPS)[:, None]
    normed = (values - average[:, None]) * inv_scale
    scaled = normed * norm_gain
    activated = jax.nn.silu(scaled).astype(jnp.bfloat16)
    grad_tokens = collect(mid_grad, "tp", 0)
    proj_grad = sum_by_axis(
        lax.dot_general(
            grad_tokens, activated, (((0,), (0,)), ((), ())), preferred_element_type=jnp.float32
        ),
        SP,
    )
    act_grad = lax.dot_general(
        grad_tokens, out_weight, (((1,), (1,)), ((), ())), preferred_element_type=jnp.float32
    )
    scaled_grad = act_grad * silu_grad(scaled) * norm_gain
    grad_total, corr_total = (
        total_of_pieces(jnp.sum(scaled_grad, axis=1), "tp"),
        total_of_pieces(jnp.sum(scaled_grad * normed, axis=1), "tp"),
    )
    grad_mean = (grad_total / model_width)[:, None]
    grad_corr = (corr_total / model_width)[:, None]
    conv_grad = (inv_scale * (scaled_grad - grad_mean - normed * grad_corr)).astype(jnp.bfloat16)
    halo_width = conv_taps.shape[0] // 2
    padded = extended(conv_grad, ((SP, 0),), halo_width)
    seq_rows = conv_grad.shape[0]
    accumulated = jnp.zeros(conv_grad.shape, jnp.float32)
    for offset in range(conv_taps.shape[0]):
        lead = 2 * halo_width - offset
        accumulated = accumulated + conv_taps[offset] * padded[lead : lead + seq_rows]
    input_grad = accumulated.astype(jnp.bfloat16)
    return (gate_grad, up_grad, down_grad, proj_grad, input_grad)


def solution(mesh):
    split = Mesh(mesh.devices.reshape(4, 4, 4, mesh.shape["tp"]), ("sp_0", "sp_1", "sp_2", "tp"))
    in_specs = (
        P(SP_TP, None),
        P(SP_TP, None),
        P(SP_TP, None),
        P(SP_TP, None),
        P(SP, "tp"),
        P(None, "tp"),
        P("tp"),
        P("tp", None),
        P(SP, None, "tp"),
        P(SP, None, "tp"),
        P(SP, "tp", None),
    )
    out_specs = (P(SP, None, "tp"), P(SP, None, "tp"), P(SP, "tp", None), P(SP, "tp"), P(SP, "tp"))
    return jax.shard_map(
        per_device, mesh=split, in_specs=in_specs, out_specs=out_specs, check_vma=False
    )
```

profile of v0, /device:TPU:0, one launch (start us, length us, event | category | flops | bytes accessed | tf_op | source)
XLA Modules:
  0.0 345.6 jit_solution(17472766416870434309)
XLA Ops:
  12.8 3.5 %gather_fusion = f32[512]{0:T(512)S(1)} fusion(f32[256]{0:T(256)S(1)} %reshape.164, s32[1024]{0:T(1024)S(1)} %pad_clamp_fusion.1), kind=kCustom, calls=%fused_computation.2 | custom fusion | bytes 6144 | tf_op jit(solution)/shard_map/jit(_take)/gather | solution.py:152
  16.4 3.3 gather_fusion.3
  19.6 3.3 gather_fusion.2
  22.9 1.9 select_bitcast_fusion
  26.7 64.1 %all_to_all.20 = bf16[64,2,8,2048]{3,2,1,0:T(8,128)(2,1)S(1)} all-to-all(bf16[64,2,8,2048]{3,2,1,0:T(8,128)(2,1)S(1)} %copy.48), channel_id=1, replica_groups=mesh['sp_0'=4,'sp_1'=4,'sp_2'=4,'tp'=2] {'sp_0','sp_1','sp_2'}, dimensions={0} | all-to-all | bytes 8388608 | tf_op jit(solution)/shard_map/all_to_all | solution.py:21
  90.7 4.3 %copy.49 = bf16[64,2,8,2048]{3,0,2,1:T(8,128)(2,1)} copy(bf16[64,2,8,2048]{3,2,1,0:T(8,128)(2,1)S(1)} %all_to_all.20) | data formatting | bytes 8388608 | tf_op jit(solution)/shard_map/all_to_all | solution.py:21
  95.1 19.5 %all-gather.10.cloned.1.call-done = bf16[128,2,8,2048]{3,0,2,1:T(8,128)(2,1)} async-done(((bf16[64,2,8,2048]{3,0,2,1:T(8,128)(2,1)}), bf16[128,2,8,2048]{3,0,2,1:T(8,128)(2,1)}) %all-gather.10.cloned.1.call-update) | async-done | bytes 8388624 | tf_op jit(solution)/shard_map/all_gather | solution.py:27
  114.6 4.7 %fusion.3 = f32[128,8,512]{2,0,1:T(8,128)S(1)} fusion(bf16[128,2,8,2048]{3,0,2,1:T(8,128)(2,1)} %all-gather.10.cloned.1.call-done, bf16[1,2048,512]{2,1,0:T(8,128)(2,1)S(1)} %copy-done), kind=kOutput, calls=%fused_computation.43 | convolution fusion | flops 2147483648 | bytes 8388608 | tf_op jit(solution)/shard_map/secd,edf->secf/dot_general | solution.py:103
  119.8 2.3 fusion.4
  122.2 3.0 fusion.40
  125.3 2.4 fusion.15
  127.7 2.4 add_convert_fusion
  130.4 8.4 %all_to_all.21 = bf16[2,64,1,8,2048]{4,1,3,2,0:T(8,128)(2,1)} all-to-all(bf16[2,64,1,8,2048]{4,1,3,2,0:T(8,128)(2,1)S(1)} %copy.55), channel_id=1, replica_groups=mesh['sp_0'=4,'sp_1'=4,'sp_2'=4,'tp'=2] {'tp'}, dimensions={0} | all-to-all | bytes 8388608 | tf_op jit(solution)/shard_map/all_to_all | solution.py:41
  138.8 3.5 %reduce_sum.111 = bf16[64,8,2048]{2,0,1:T(8,128)(2,1)S(1)} reduce(bf16[2,64,1,8,2048]{4,1,3,2,0:T(8,128)(2,1)} %all_to_all.21, bf16[]{:T(256)} %constant.78.clone.1), dimensions={0,2}, to_apply=%region_4.6 | reduce | flops 1048576 | bytes 6291458 | tf_op jit(solution)/shard_map/reduce_sum | solution.py:42
  142.3 2.5 copy.57
  144.7 10.5 %all-to-all-start.2 = ((bf16[64,1,8,2048]{3,2,1,0:T(8,128)(2,1)}), bf16[64,1,8,2048]{3,2,1,0:T(8,128)(2,1)S(1)}, u32[]{:S(2)}, u32[]{:S(2)}) async-start(bf16[64,1,8,2048]{3,2,1,0:T(8,128)(2,1)} %copy.57), calls=%async_computation.2 | async-start | bytes 4194304 | tf_op jit(solution)/shard_map/all_to_all | solution.py:166
  155.7 1.8 all-gather.5
  157.5 1.8 all-gather.4
  159.6 26.0 %all-to-all-done.2 = bf16[64,1,8,2048]{3,2,1,0:T(8,128)(2,1)S(1)} async-done(((bf16[64,1,8,2048]{3,2,1,0:T(8,128)(2,1)}), bf16[64,1,8,2048]{3,2,1,0:T(8,128)(2,1)S(1)}, u32[]{:S(2)}, u32[]{:S(2)}) %all-to-all-start.2) | async-done | bytes 2097184 | tf_op jit(solution)/shard_map/all_to_all | solution.py:166
  185.6 2.3 gather_fusion.1
  189.7 3.8 %convert_reduce_fusion = f32[128,2048]{1,0:T(8,128)S(1)} fusion(bf16[128,2,2048]{2,1,0:T(2,128)(2,1)S(1)} %gather.15, pred[128,2]{1,0:T(8,128)(4,1)S(1)} %copy.54), kind=kLoop, calls=%fused_computation.68 | loop fusion | flops 1310720 | bytes 2097408 | tf_op jit(solution)/shard_map/reduce_sum | solution.py:170
  193.8 4.6 %all_to_all.22 = bf16[2,128,2048]{2,1,0:T(8,128)(2,1)S(1)} all-to-all(bf16[2,128,2048]{2,1,0:T(8,128)(2,1)S(1)} %broadcast_in_dim.47), channel_id=1, replica_groups=mesh['sp_0'=4,'sp_1'=4,'sp_2'=4,'tp'=2] {'tp'}, dimensions={0} | all-to-all | bytes 2097152 | tf_op jit(solution)/shard_map/all_to_all | solution.py:53
  198.4 4.8 %fusion.45 = f32[2048,1024]{1,0:T(8,128)} fusion(bf16[256,2048]{1,0:T(8,128)(2,1)S(1)} %bitcast.185, bf16[256,1024]{1,0:T(8,128)(2,1)S(1)} %copy-done.5, f32[1024]{0:T(1024)S(1)} %copy-done.8, f32[256]{0:T(256)S(1)} %get-tuple-element.48, f32[256]{0:T(256)S(1)} %get-tuple-element.47), kind=kOutput, calls=%fused_computation.99 | convolution fusion | flops 1076101120 | bytes 9967616 | tf_op jit(solution)/shard_map/dot_general | solution.py:182
  203.3 77.5 %reduce-scatter.4.cloned.1.call-done = f32[512,1024]{1,0:T(8,128)} async-done(((f32[2048,1024]{1,0:T(8,128)}), f32[512,1024]{1,0:T(8,128)}) %reduce-scatter.4.cloned.1.call-update) | async-done | bytes 2097168 | tf_op jit(solution)/shard_map/reduce_scatter | solution.py:62
  281.3 6.7 %convolution_bitcast_fusion = f32[1,2048,512]{2,1,0:T(8,128)} fusion(bf16[128,8,512]{2,0,1:T(8,128)(2,1)S(1)} %copy-done.14, bf16[128,2,8,2048]{3,0,2,1:T(8,128)(2,1)} %all-gather.10.cloned.1.call-done), kind=kOutput, calls=%fused_computation.13 | convolution fusion | flops 2147483648 | bytes 9437184 | tf_op jit(solution)/shard_map/secd,secf->edf/dot_general | solution.py:112
  288.0 6.8 %fusion.2 = f32[1,512,2048]{2,1,0:T(8,128)} fusion(bf16[128,2,8,2048]{3,0,2,1:T(8,128)(2,1)} %all-gather.10.cloned.1.call-done, f32[128,8,512]{2,0,1:T(8,128)S(1)} %copy-done.19, f32[128,8,512]{2,0,1:T(8,128)S(1)} %copy-done.17), kind=kOutput, calls=%fused_computation.12 | convolution fusion | flops 2150629376 | bytes 12582912 | tf_op jit(solution)/shard_map/secf,secd->efd/dot_general | solution.py:107
  296.6 1.8 all-gather.7
  298.4 1.8 all-gather.6
  301.9 4.5 %collective-permute-start.1 = (bf16[15,1024]{1,0:T(8,128)(2,1)S(1)}, bf16[15,1024]{1,0:T(8,128)(2,1)S(1)}, u32[]{:S(2)}, u32[]{:S(2)}) collective-permute-start(bf16[15,1024]{1,0:T(8,128)(2,1)S(1)} %get-tuple-element.15), channel_id=1, source_target_pairs={{0,2},{2,4},{4,6},{6,8},{8,10},{10,12},{12,14},{14,16},{16,18},{18... | collective-permute-start | bytes 92168 | tf_op jit(solution)/shard_map/ppermute | solution.py:71
  306.5 7.1 %convolution_bitcast_fusion.1 = f32[1,2048,512]{2,1,0:T(8,128)} fusion(bf16[128,2,8,2048]{3,0,2,1:T(8,128)(2,1)} %all-gather.10.cloned.1.call-done, bf16[128,1,8,512]{3,0,2,1:T(8,128)(2,1)} %copy-done.15), kind=kOutput, calls=%fused_computation.14 | convolution fusion | flops 2147483648 | bytes 9437184 | tf_op jit(solution)/shard_map/secd,secf->edf/dot_general | solution.py:111
  313.6 5.5 %add_convert_fusion.1 = bf16[256,1024]{1,0:T(8,128)(2,1)} fusion(bf16[256,1024]{1,0:T(8,128)(2,1)S(1)} %fusion.38, bf16[15,1024]{1,0:T(8,128)(2,1)S(1)} %collective-permute-done.1, bf16[15,1024]{1,0:T(8,128)(2,1)S(1)} %collective-permute-done, f32[1024]{0:T(1024)S(1)} %bitcast.198, f32[1024]{0:T(1024)S(1)} %bitcast.199, f32[1024]{0:T(1024)S(1)} %bitcast.201, ...), kind=kLoop, calls=%fused_computation.97 | loop fusion | flops 47972352 | bytes 1236992 | tf_op jit(solution)/shard_map/convert_element_type | solution.py:205
  319.1 19.5 %reduce-scatter.8.cloned.1.call-done = f32[32,1024]{1,0:T(8,128)} async-done(((f32[128,1024]{1,0:T(8,128)}), f32[32,1024]{1,0:T(8,128)}) %reduce-scatter.8.cloned.1.call-update) | async-done | bytes 131088 | tf_op jit(solution)/shard_map/reduce_scatter | solution.py:62
  (99 shorter events, 14.9 us)
Async XLA Ops:
  7.2 107.4 %copy-start = (bf16[1,2048,512]{2,1,0:T(8,128)(2,1)S(1)}, bf16[1,2048,512]{2,1,0:T(8,128)(2,1)}, u32[]{:S(2)}) copy-start(bf16[1,2048,512]{2,1,0:T(8,128)(2,1)} %param.21) | copy-start | bytes 6291460
  7.2 9.2 %copy-start.2 = (bf16[128,2048]{1,0:T(8,128)(2,1)S(1)}, bf16[128,2048]{1,0:T(8,128)(2,1)}, u32[]{:S(2)}) copy-start(bf16[128,2048]{1,0:T(8,128)(2,1)} %param.14) | copy-start | bytes 1572868
  7.2 107.4 %all-gather.10.cloned.1.call-start = ((), (), s32[]{:S(2)}) async-start(), calls=%async_computation.7 | async-start | bytes 12582912 | tf_op jit(solution)/shard_map/all_gather | solution.py:27
  16.3 3.3 copy-start.3
  22.9 2.2 copy-start.4
  114.6 4.7 %copy-start.9 = (bf16[128,2,8,2048]{3,0,2,1:T(8,128)(2,1)S(1)}, bf16[128,2,8,2048]{3,0,2,1:T(8,128)(2,1)}, u32[]{:S(2)}) copy-start(bf16[128,2,8,2048]{3,0,2,1:T(8,128)(2,1)} %all-gather.10.cloned.1.call-done) | copy-start | bytes 25165828
  114.6 5.2 %copy-start.12 = (bf16[1,2048,512]{2,1,0:T(8,128)(2,1)S(1)}, bf16[1,2048,512]{2,1,0:T(8,128)(2,1)}, u32[]{:S(2)}) copy-start(bf16[1,2048,512]{2,1,0:T(8,128)(2,1)} %param.22) | copy-start | bytes 6291460
  119.8 2.3 copy-start.16
  119.8 2.3 copy-start.11
  122.2 3.0 copy-start.18
  125.2 2.4 copy-start.15
  125.3 2.4 copy-start.13
  144.7 10.7 %copy-start.5 = (bf16[256,1024]{1,0:T(8,128)(2,1)S(1)}, bf16[256,1024]{1,0:T(8,128)(2,1)}, u32[]{:S(2)}) copy-start(bf16[256,1024]{1,0:T(8,128)(2,1)} %param.17) | copy-start | bytes 1572868
  144.7 14.7 %copy-start.7 = (s32[128,2]{0,1:T(2,128)S(1)}, s32[128,2]{0,1:T(2,128)}, u32[]{:S(2)}) copy-start(s32[128,2]{0,1:T(2,128)} %param.15) | copy-start | bytes 3076
  144.7 40.9 %all-to-all-start.2 = ((bf16[64,1,8,2048]{3,2,1,0:T(8,128)(2,1)}), bf16[64,1,8,2048]{3,2,1,0:T(8,128)(2,1)S(1)}, u32[]{:S(2)}, u32[]{:S(2)}) async-start(bf16[64,1,8,2048]{3,2,1,0:T(8,128)(2,1)} %copy.57), calls=%async_computation.2 | async-start | bytes 4194304 | tf_op jit(solution)/shard_map/all_to_all | solution.py:166
  155.3 125.5 %reduce-scatter.4.cloned.1.call-start = ((), (), s32[]{:S(2)}) async-start(), calls=%async_computation.8 | async-start | bytes 10485760 | tf_op jit(solution)/shard_map/reduce_scatter | solution.py:62
  193.7 4.7 %copy-start.8 = (f32[1024]{0:T(1024)S(1)}, f32[1024]{0:T(1024)}, u32[]{:S(2)}) copy-start(f32[1024]{0:T(1024)} %param.19) | copy-start | bytes 12292
  203.2 77.9 %copy-start.6 = (f32[31,1024]{1,0:T(8,128)S(1)}, f32[31,1024]{1,0:T(8,128)}, u32[]{:S(2)}) copy-start(f32[31,1024]{1,0:T(8,128)} %param.18) | copy-start | bytes 380932
  203.2 78.0 %copy-start.14 = (bf16[128,8,512]{2,0,1:T(8,128)(2,1)S(1)}, bf16[128,8,512]{2,0,1:T(8,128)(2,1)}, u32[]{:S(2)}) copy-start(bf16[128,8,512]{2,0,1:T(8,128)(2,1)} %copy-done.13) | copy-start | bytes 3145732
  203.3 110.3 %reduce-scatter.6.cloned.1.call-start = ((), (), s32[]{:S(2)}) async-start(), calls=%async_computation.9 | async-start | bytes 2621440 | tf_op jit(solution)/shard_map/reduce_scatter | solution.py:62
  280.8 57.8 %reduce-scatter.8.cloned.1.call-start = ((), (), s32[]{:S(2)}) async-start(), calls=%async_computation.10 | async-start | bytes 655360 | tf_op jit(solution)/shard_map/reduce_scatter | solution.py:62
  281.3 6.8 %copy-start.17 = (f32[128,8,512]{2,0,1:T(8,128)S(1)}, f32[128,8,512]{2,0,1:T(8,128)}, u32[]{:S(2)}) copy-start(f32[128,8,512]{2,0,1:T(8,128)} %copy-done.16) | copy-start | bytes 6291460
  281.3 6.8 %copy-start.19 = (f32[128,8,512]{2,0,1:T(8,128)S(1)}, f32[128,8,512]{2,0,1:T(8,128)}, u32[]{:S(2)}) copy-start(f32[128,8,512]{2,0,1:T(8,128)} %copy-done.18) | copy-start | bytes 6291460
  288.0 6.8 %copy-start.10 = (bf16[1024,2048]{1,0:T(8,128)(2,1)S(1)}, bf16[1024,2048]{1,0:T(8,128)(2,1)}, u32[]{:S(2)}) copy-start(bf16[1024,2048]{1,0:T(8,128)(2,1)} %param.20) | copy-start | bytes 12582916
  300.6 13.0 %collective-permute-start = (bf16[15,1024]{1,0:T(8,128)(2,1)S(1)}, bf16[15,1024]{1,0:T(8,128)(2,1)S(1)}, u32[]{:S(2)}, u32[]{:S(2)}) collective-permute-start(bf16[15,1024]{1,0:T(8,128)(2,1)S(1)} %get-tuple-element.14), channel_id=1, source_target_pairs={{2,0},{4,2},{6,4},{8,6},{10,8},{12,10},{14,12},{16,14},{18,16},{20... | collective-permute-start | bytes 92168 | tf_op jit(solution)/shard_map/ppermute | solution.py:74
  301.9 11.7 %collective-permute-start.1 = (bf16[15,1024]{1,0:T(8,128)(2,1)S(1)}, bf16[15,1024]{1,0:T(8,128)(2,1)S(1)}, u32[]{:S(2)}, u32[]{:S(2)}) collective-permute-start(bf16[15,1024]{1,0:T(8,128)(2,1)S(1)} %get-tuple-element.15), channel_id=1, source_target_pairs={{0,2},{2,4},{4,6},{6,8},{8,10},{10,12},{12,14},{14,16},{16,18},{18... | collective-permute-start | bytes 92168 | tf_op jit(solution)/shard_map/ppermute | solution.py:71
  306.5 32.1 %copy-start.1 = (bf16[1,2048,512]{2,1,0:T(8,128)(2,1)S(1)}, bf16[1,2048,512]{2,1,0:T(8,128)(2,1)}, u32[]{:S(2)}) copy-start(bf16[1,2048,512]{2,1,0:T(8,128)(2,1)} %param.21) | copy-start | bytes 6291460
Sparse Core Ops, SparseCore 0:
  95.2 19.3 all-gather.9
  203.4 77.4 reduce-scatter.3
  283.2 29.2 reduce-scatter.5
  315.4 23.1 reduce-scatter.7
where the time goes:
time: 351 us; the launch traced here: 346 us
  waiting for transfers between devices  143 us (41%)
  blocking collectives  84.3 us (24%)
  matrix products  41.9 us (12%)
  local copies, waits for them, and re-layouts  27.1 us (8%)
  other arithmetic  18.2 us (5%)
  starting transfers between devices  16.8 us (5%)
  between operations  14.7 us (4%)
    reduce_scatter x3, waiting for transfers between devices, sum_by_axis(): so_far = lax.psum_scatter(so_far, axis, scatter_dimension=0, tiled=True)  97 us
    all_to_all x1, blocking collectives, sent_together(): lax.all_to_all(both, axis, split_axis=split_dim, concat_axis=concat_dim,...  64.1 us
    all_to_all x1, waiting for transfers between devices, per_device(): lax.all_to_all(back_rows, SP, split_axis=0, concat_axis=0, tiled=True)  26 us
    all_gather x1, waiting for transfers between devices, sent_together_2(): lax.all_gather(both, axis, axis=dim, tiled=True)  19.5 us
    all_to_all x1, starting transfers between devices, per_device(): lax.all_to_all(back_rows, SP, split_axis=0, concat_axis=0, tiled=True)  10.5 us
    all_to_all x1, blocking collectives, sent_and_summed(): lax.all_to_all(pieces, axis, split_axis=0, concat_axis=0, tiled=True)  8.41 us
    all_gather x4, blocking collectives, total_of_pieces(): return lax.all_gather(value, axis).sum(0)  7.21 us
    dot_general x1, matrix products, expert_backward(): jnp.einsum('secd,secf->edf', inputs, gate_pre, preferred_element_type=jnp...  7.05 us
  transfers between devices with their start and end apart: 7, of which 4 were waited for; matrix products, arithmetic and copies ran while one was open for 8% of the time, Pallas kernels for 0%

commit v1 on v0

v1 whole, which is shorter than its diff:
```python
import jax
import jax.numpy as jnp
from jax import lax
from jax.sharding import Mesh
from jax.sharding import PartitionSpec as P

SP = ("sp_0", "sp_1", "sp_2")
SP_TP = ("sp_0", "sp_1", "sp_2", "tp")
NORM_EPS = 1e-05
CAPACITY = 8
SWAP = [(0, 1), (1, 0)]


def dot_f32(a, b, dims):
    return lax.dot_general(a, b, (dims, ((), ())), preferred_element_type=jnp.float32)


def silu_grad(pre_act):
    logistic = jax.nn.sigmoid(pre_act)
    return logistic * (1.0 + pre_act * (1.0 - logistic))


def swapped(value):
    return lax.ppermute(value, "tp", SWAP)


def selection(routes, route_weight, experts):
    rows = routes.shape[0]
    ids = lax.broadcasted_iota(jnp.int32, (experts, rows), 0)
    hits = [ids == routes[:, k][None, :] for k in range(routes.shape[1])]
    named = sum(h.astype(jnp.float32) for h in hits)
    weight = sum(
        jnp.where(h, route_weight[:, k][None, :], 0.0) for k, h in enumerate(hits)
    )
    earlier = lax.broadcasted_iota(jnp.int32, (rows, rows), 0) < lax.broadcasted_iota(
        jnp.int32, (rows, rows), 1
    )
    place = dot_f32(named.astype(jnp.bfloat16), earlier.astype(jnp.bfloat16), ((1,), (0,)))
    slot = lax.broadcasted_iota(jnp.int32, (experts, CAPACITY, rows), 1).astype(jnp.float32)
    chosen = (place[:, None, :] == slot) & (named[:, None, :] > 0.0)
    scale = jnp.sum(jnp.where(chosen, weight[:, None, :], 0.0), axis=2)
    matrix = chosen.astype(jnp.bfloat16).reshape(experts * CAPACITY, rows)
    return matrix, scale.reshape(experts * CAPACITY)


def per_device(
    mid_rows,
    cotangent,
    routes,
    route_weight,
    filtered,
    conv_taps,
    norm_gain,
    out_weight,
    gate_weight,
    up_weight,
    down_weight,
):
    sp_count = lax.axis_size(SP)
    width = mid_rows.shape[1]
    gate_mat, up_mat, down_mat = gate_weight[0], up_weight[0], down_weight[0]

    matrix, scale = selection(routes, route_weight, sp_count)
    inputs = dot_f32(matrix, mid_rows, ((1,), (0,))).astype(jnp.bfloat16)
    cot_rows = dot_f32(matrix, cotangent, ((1,), (0,)))
    routed = (scale[:, None] * cot_rows).astype(jnp.bfloat16)
    both = jnp.concatenate((inputs, routed), axis=1).reshape(sp_count, CAPACITY, 2 * width)
    arrived = lax.all_to_all(both, SP, split_axis=0, concat_axis=0, tiled=True)
    arrived = arrived.reshape(sp_count * CAPACITY, 2 * width)
    partner = swapped(arrived)
    all_rows = jnp.concatenate((partner, arrived), axis=0)
    all_in, all_cot = all_rows[:, :width], all_rows[:, width:]

    pre_gate = dot_f32(all_in, gate_mat, ((1,), (0,)))
    pre_up = dot_f32(all_in, up_mat, ((1,), (0,)))
    gate_act = jax.nn.silu(pre_gate)
    hidden = (gate_act * pre_up).astype(jnp.bfloat16)
    hidden_grad = dot_f32(all_cot, down_mat, ((1,), (1,)))
    gate_pre = (hidden_grad * pre_up * silu_grad(pre_gate)).astype(jnp.bfloat16)
    up_pre = (hidden_grad * gate_act).astype(jnp.bfloat16)
    half = sp_count * CAPACITY

    def part(rows):
        return (
            dot_f32(gate_pre[rows], gate_mat, ((1,), (1,)))
            + dot_f32(up_pre[rows], up_mat, ((1,), (1,)))
        ).astype(jnp.bfloat16)

    from_partner = swapped(part(slice(0, half)))
    kept = part(slice(half, 2 * half))
    back = (kept.astype(jnp.float32) + from_partner.astype(jnp.float32)).astype(jnp.bfloat16)
    returned = lax.all_to_all(
        back.reshape(sp_count, CAPACITY, width), SP, split_axis=0, concat_axis=0, tiled=True
    ).reshape(half, width)

    gate_grad = dot_f32(all_in, gate_pre, ((0,), (0,)))[None]
    up_grad = dot_f32(all_in, up_pre, ((0,), (0,)))[None]
    down_grad = dot_f32(hidden, all_cot, ((0,), (0,)))[None]

    route_sum = dot_f32(matrix, returned, ((0,), (0,)))
    mid_grad = (cotangent.astype(jnp.float32) + route_sum).astype(jnp.bfloat16)
    other = swapped(mid_grad)
    first = lax.axis_index("tp") == 0
    grad_tokens = jnp.concatenate(
        (jnp.where(first, mid_grad, other), jnp.where(first, other, mid_grad)), axis=0
    )

    values = filtered.astype(jnp.float32)
    sums = jnp.stack((jnp.sum(values, axis=1), jnp.sum(values * values, axis=1)))
    sums = sums + swapped(sums)
    average = sums[0] / width
    variance = sums[1] / width - average * average
    inv_scale = lax.rsqrt(variance + NORM_EPS)[:, None]
    normed = (values - average[:, None]) * inv_scale
    scaled = normed * norm_gain
    activated = jax.nn.silu(scaled).astype(jnp.bfloat16)

    partial = dot_f32(grad_tokens, activated, ((0,), (0,))).astype(jnp.bfloat16)
    pieces = lax.all_to_all(
        partial.reshape(sp_count, width // sp_count, partial.shape[1]),
        SP,
        split_axis=0,
        concat_axis=0,
        tiled=True,
    )
    proj_grad = jnp.sum(pieces.astype(jnp.float32), axis=0)

    act_grad = dot_f32(grad_tokens, out_weight, ((1,), (1,)))
    scaled_grad = act_grad * silu_grad(scaled) * norm_gain
    totals = jnp.stack((jnp.sum(scaled_grad, axis=1), jnp.sum(scaled_grad * normed, axis=1)))
    totals = totals + swapped(totals)
    grad_mean = (totals[0] / width)[:, None]
    grad_corr = (totals[1] / width)[:, None]
    conv_grad = (inv_scale * (scaled_grad - grad_mean - normed * grad_corr)).astype(jnp.bfloat16)

    taps = conv_taps.shape[0]
    reach = taps // 2
    rows = conv_grad.shape[0]
    low = lax.ppermute(
        conv_grad[rows - reach :], SP, [(i, i + 1) for i in range(sp_count - 1)]
    )
    high = lax.ppermute(conv_grad[:reach], SP, [(i + 1, i) for i in range(sp_count - 1)])
    padded = jnp.concatenate((low, conv_grad, high), axis=0)
    accumulated = jnp.zeros(conv_grad.shape, jnp.float32)
    for offset in range(taps):
        lead = 2 * reach - offset
        accumulated = accumulated + conv_taps[offset] * padded[lead : lead + rows]
    input_grad = accumulated.astype(jnp.bfloat16)
    return (gate_grad, up_grad, down_grad, proj_grad, input_grad)


def solution(mesh):
    split = Mesh(mesh.devices.reshape(4, 4, 4, mesh.shape["tp"]), ("sp_0", "sp_1", "sp_2", "tp"))
    in_specs = (
        P(SP_TP, None),
        P(SP_TP, None),
        P(SP_TP, None),
        P(SP_TP, None),
        P(SP, "tp"),
        P(None, "tp"),
        P("tp"),
        P("tp", None),
        P(SP, None, "tp"),
        P(SP, None, "tp"),
        P(SP, "tp", None),
    )
    out_specs = (P(SP, None, "tp"), P(SP, None, "tp"), P(SP, "tp", None), P(SP, "tp"), P(SP, "tp"))
    return jax.shard_map(
        per_device, mesh=split, in_specs=in_specs, out_specs=out_specs, check_vma=False
    )
```

time: 351 us -> 209 us (0.60)
  waiting for transfers between devices: 143 us -> 64.6 us
  local copies, waits for them, and re-layouts: 27.1 us -> 3.1 us
  blocking collectives: 84.3 us -> 63.9 us
  between operations: 14.7 us -> 1.05 us
  other arithmetic: 18.2 us -> 12 us
    reduce_scatter x3 -> x0, waiting for transfers between devices: 97 us -> none  [sum_by_axis(): so_far = lax.psum_scatter(so_far, axis, scatter_dimension=0, tiled=True)]
    ppermute x2 -> x7, waiting for transfers between devices: 0.01 us -> 35.7 us  [the longest x1 24 us: per_device(): lax.ppermute(conv_grad[:reach], SP, [(i + 1, i) for i in range(sp_count -...]
    all_gather x1 -> x0, waiting for transfers between devices: 19.5 us -> none  [sent_together_2(): lax.all_gather(both, axis, axis=dim, tiled=True)]
    gather x5 -> x0, local copies, waits for them, and re-layouts: 14.1 us -> none  [the longest x2 4.07 us: per_device(): route_rows = jnp.take(back_all, target, axis=0)]
    all_to_all x3 -> x1, blocking collectives: 77 us -> 63.9 us  [per_device(): arrived = lax.all_to_all(both, SP, split_axis=0, concat_axis=0, tiled=True)]
    all_gather x4 -> x0, blocking collectives: 7.21 us -> none  [total_of_pieces(): return lax.all_gather(value, axis).sum(0)]
    all_to_all x1 -> x0, local copies, waits for them, and re-layouts: 4.31 us -> none  [sent_together(): lax.all_to_all(both, axis, split_axis=split_dim, concat_axis=concat_dim,...]
    reduce_sum x7 -> x2, other arithmetic: 7.5 us -> 3.9 us  [the longest x1 3.68 us: per_device(): proj_grad = jnp.sum(pieces.astype(jnp.float32), axis=0)]
  transfers between devices with their start and end apart: 7 -> 9, of which waited for: 4 -> 5; matrix products, arithmetic and copies ran while one was open for 8% -> 14% of each run, Pallas kernels for 0% -> 0%
where the time goes in v1:
time: 209 us; the launch traced here: 207 us
  waiting for transfers between devices  64.6 us (31%)
  blocking collectives  63.9 us (31%)
  matrix products  43.2 us (21%)
  starting transfers between devices  18.7 us (9%)
  other arithmetic  12 us (6%)
  local copies, waits for them, and re-layouts  3.1 us (1%)
    all_to_all x1, blocking collectives, per_device(): arrived = lax.all_to_all(both, SP, split_axis=0, concat_axis=0, tiled=True)  63.9 us
    dot_general x16, matrix products, dot_f32(): lax.dot_general(a, b, (dims, ((), ())), preferred_element_type=jnp.float32)  43.2 us
    all_to_all x1, waiting for transfers between devices, per_device(): lax.all_to_all(back.reshape(sp_count, CAPACITY, width), SP, split_axis=0,...  28.9 us
    ppermute x1, waiting for transfers between devices, per_device(): lax.ppermute(conv_grad[:reach], SP, [(i + 1, i) for i in range(sp_count -...  24 us
    ppermute x5, waiting for transfers between devices, swapped(): return lax.ppermute(value, 'tp', SWAP)  11.7 us
    all_to_all x1, starting transfers between devices, per_device(): lax.all_to_all(back.reshape(sp_count, CAPACITY, width), SP, split_axis=0,...  6.04 us
    all_to_all x1, starting transfers between devices, per_device(): lax.all_to_all(partial.reshape(sp_count, width // sp_count, partial.shape...  5.97 us
    convert_element_type x1, other arithmetic, per_device(): input_grad = accumulated.astype(jnp.bfloat16)  5.43 us
  transfers between devices with their start and end apart: 9, of which 5 were waited for; matrix products, arithmetic and copies ran while one was open for 14% of the time, Pallas kernels for 0%

profile of v1, /device:TPU:0, one launch (start us, length us, event | category | flops | bytes accessed | tf_op | source)
XLA Modules:
  0.0 206.6 jit_solution(89909433127757036)
XLA Ops:
  0.7 0.8 slice_bitcast_fusion.3
  1.7 0.8 slice_bitcast_fusion.1
  2.9 1.8 convolution_convert_fusion.1
  4.7 1.8 multiply_convert_fusion
  6.5 0.5 maximum_bitcast_fusion
  6.9 63.9 %all_to_all.15 = bf16[64,8,4096]{2,1,0:T(8,128)(2,1)S(1)} all-to-all(bf16[64,8,4096]{2,1,0:T(8,128)(2,1)S(1)} %maximum_bitcast_fusion), channel_id=1, replica_groups=mesh['sp_0'=4,'sp_1'=4,'sp_2'=4,'tp'=2] {'sp_0','sp_1','sp_2'}, dimensions={0} | all-to-all | bytes 8388608 | tf_op jit(solution)/shard_map/all_to_all | solution.py:68
  70.8 7.2 %collective-permute-done = bf16[512,4096]{1,0:T(8,128)(2,1)S(1)} collective-permute-done((bf16[512,4096]{1,0:T(8,128)(2,1)S(1)}, bf16[512,4096]{1,0:T(8,128)(2,1)S(1)}, u32[]{:S(2)}, u32[]{:S(2)}) %collective-permute-start) | collective-permute-done | bytes 4194336 | tf_op jit(solution)/shard_map/ppermute | solution.py:24
  78.4 2.3 %fusion.8 = f32[1024,512]{1,0:T(8,128)S(1)} fusion(bf16[1024,2048]{1,0:T(8,128)(2,1)S(1)} %fusion, bf16[1,2048,512]{2,1,0:T(8,128)(2,1)S(1)} %copy-done), kind=kOutput, calls=%fused_computation.51 | convolution fusion | flops 2147483648 | bytes 8388608 | tf_op jit(solution)/shard_map/dot_general | solution.py:15
  80.7 0.7 copy-done.3
  81.5 2.3 %fusion.12 = f32[1024,512]{1,0:T(8,128)S(1)} fusion(bf16[1024,2048]{1,0:T(8,128)(2,1)S(1)} %fusion, bf16[1,2048,512]{2,1,0:T(8,128)(2,1)S(1)} %copy-done.3), kind=kOutput, calls=%fused_computation.55 | convolution fusion | flops 2147483648 | bytes 8388608 | tf_op jit(solution)/shard_map/dot_general | solution.py:15
  83.8 4.4 %multiply_convert_fusion.2 = (bf16[1024,512]{1,0:T(8,128)(2,1)S(1)}, bf16[1024,512]{1,0:T(8,128)(2,1)S(1)}) fusion(f32[1024,512]{1,0:T(8,128)S(1)} %fusion.8, f32[1024,512]{1,0:T(8,128)S(1)} %fusion.12, bf16[1,512,2048]{2,1,0:T(8,128)(2,1)S(1)} %copy-done.15, bf16[512,4096]{1,0:T(8,128)(2,1)S(1)} %bitcast.106, bf16[512,4096]{1,0:T(8,128)(2,1)S(1)} %collective-permute-done), kind=kOutput, calls=%fused_computation.60 | convolution fusion | flops 2162688000 | bytes 16777216 | tf_op jit(solution)/shard_map/dot_general | solution.py:15
  88.2 1.3 fusion.4
  89.5 1.3 add_convert_fusion.1
  91.2 1.3 fusion.6
  92.5 2.7 %collective-permute-done.1 = bf16[512,2048]{1,0:T(8,128)(2,1)S(1)} collective-permute-done((bf16[512,2048]{1,0:T(8,128)(2,1)S(1)}, bf16[512,2048]{1,0:T(8,128)(2,1)S(1)}, u32[]{:S(2)}, u32[]{:S(2)}) %collective-permute-start.1) | collective-permute-done | bytes 2097184 | tf_op jit(solution)/shard_map/ppermute | solution.py:24
  95.3 2.7 %fusion.1 = bf16[64,8,2048]{2,1,0:T(8,128)(2,1)} fusion(bf16[512,2048]{1,0:T(8,128)(2,1)S(1)} %collective-permute-done.1, f32[512,2048]{1,0:T(8,128)S(1)} %fusion.6, bf16[1,2048,512]{2,1,0:T(8,128)(2,1)S(1)} %copy-done.3, bf16[1024,512]{1,0:T(8,128)(2,1)S(1)} %get-tuple-element.9), kind=kOutput, calls=%fused_computation.43 | convolution fusion | flops 1080033280 | bytes 11010048 | tf_op jit(solution)/shard_map/dot_general | solution.py:15
  98.0 6.0 %all-to-all-start.1 = ((bf16[64,8,2048]{2,1,0:T(8,128)(2,1)}), bf16[64,8,2048]{2,1,0:T(8,128)(2,1)S(1)}, u32[]{:S(2)}, u32[]{:S(2)}) async-start(bf16[64,8,2048]{2,1,0:T(8,128)(2,1)} %fusion.1), calls=%async_computation.1 | async-start | bytes 4194304 | tf_op jit(solution)/shard_map/all_to_all | solution.py:92
  104.0 1.3 convert_reduce_fusion.1
  105.5 28.9 %all-to-all-done.1 = bf16[64,8,2048]{2,1,0:T(8,128)(2,1)S(1)} async-done(((bf16[64,8,2048]{2,1,0:T(8,128)(2,1)}), bf16[64,8,2048]{2,1,0:T(8,128)(2,1)S(1)}, u32[]{:S(2)}, u32[]{:S(2)}) %all-to-all-start.1) | async-done | bytes 2097184 | tf_op jit(solution)/shard_map/all_to_all | solution.py:92
  134.4 1.7 fusion.3
  136.2 1.8 collective-permute-done.2
  138.2 3.6 %convolution_convert_fusion = bf16[2048,1024]{1,0:T(8,128)(2,1)} fusion(bf16[128,2048]{1,0:T(8,128)(2,1)S(1)} %get-tuple-element.12, bf16[128,2048]{1,0:T(8,128)(2,1)S(1)} %get-tuple-element.11, bf16[256,1024]{1,0:T(8,128)(2,1)S(1)} %copy-done.7, f32[1024]{0:T(1024)S(1)} %copy-done.16, f32[256]{0:T(256)S(1)} %add_rsqrt_fusion, f32[256]{0:T(256)S(1)} %bitcast.141), kind=kOutput, calls=%fused_computation.10 | convolution fusion | flops 1080295424 | bytes 5773312 | tf_op jit(solution)/shard_map/dot_general | solution.py:15
  141.8 6.0 %all-to-all-start.2 = ((bf16[64,32,1024]{2,1,0:T(8,128)(2,1)}), bf16[64,32,1024]{2,1,0:T(8,128)(2,1)}, u32[]{:S(2)}, u32[]{:S(2)}) async-start(bf16[64,32,1024]{2,1,0:T(8,128)(2,1)} %bitcast.108), calls=%async_computation.2 | async-start | bytes 8388608 | tf_op jit(solution)/shard_map/all_to_all | solution.py:119
  147.8 8.1 %convolution_bitcast_fusion = f32[1,512,2048]{2,1,0:T(8,128)} fusion(f32[1024,512]{1,0:T(8,128)} %copy-done.18, bf16[512,4096]{1,0:T(8,128)(2,1)} %bitcast.107, bf16[512,4096]{1,0:T(8,128)(2,1)} %copy-done.6, f32[1024,512]{1,0:T(8,128)} %copy-done.17), kind=kOutput, calls=%fused_computation.11 | convolution fusion | flops 2159017984 | bytes 16777216 | tf_op jit(solution)/shard_map/dot_general | solution.py:15
  156.0 1.7 fusion.100
  158.4 4.4 %convolution_bitcast_fusion.1 = f32[1,2048,512]{2,1,0:T(8,128)} fusion(bf16[1024,2048]{1,0:T(8,128)(2,1)S(1)} %copy-done.5, bf16[1024,512]{1,0:T(8,128)(2,1)S(1)} %copy-done.10), kind=kOutput, calls=%fused_computation.12 | convolution fusion | flops 2147483648 | bytes 9437184 | tf_op jit(solution)/shard_map/dot_general | solution.py:15
  163.2 1.3 collective-permute-start.5
  164.5 4.5 %collective-permute-start.6 = (bf16[15,1024]{1,0:T(8,128)(2,1)S(1)}, bf16[15,1024]{1,0:T(8,128)(2,1)S(1)}, u32[]{:S(2)}, u32[]{:S(2)}) collective-permute-start(bf16[15,1024]{1,0:T(8,128)(2,1)S(1)} %get-tuple-element.14), channel_id=1, source_target_pairs={{0,2},{2,4},{4,6},{6,8},{8,10},{10,12},{12,14},{14,16},{16,18},{18... | collective-permute-start | bytes 92168 | tf_op jit(solution)/shard_map/ppermute | solution.py:139
  169.1 4.4 %convolution_bitcast_fusion.2 = f32[1,2048,512]{2,1,0:T(8,128)} fusion(bf16[1024,2048]{1,0:T(8,128)(2,1)S(1)} %copy-done.5, bf16[1024,512]{1,0:T(8,128)(2,1)S(1)} %get-tuple-element.10), kind=kOutput, calls=%fused_computation.13 | convolution fusion | flops 2147483648 | bytes 9437184 | tf_op jit(solution)/shard_map/dot_general | solution.py:15
  173.5 24.0 %collective-permute-done.5 = bf16[15,1024]{1,0:T(8,128)(2,1)S(1)} collective-permute-done((bf16[15,1024]{1,0:T(8,128)(2,1)S(1)}, bf16[15,1024]{1,0:T(8,128)(2,1)S(1)}, u32[]{:S(2)}, u32[]{:S(2)}) %collective-permute-start.5) | collective-permute-done | bytes 30752 | tf_op jit(solution)/shard_map/ppermute | solution.py:142
  197.5 5.4 %add_convert_fusion.3 = bf16[256,1024]{1,0:T(8,128)(2,1)} fusion(bf16[256,1024]{1,0:T(8,128)(2,1)S(1)} %fusion.35, bf16[15,1024]{1,0:T(8,128)(2,1)S(1)} %collective-permute-done.6, bf16[15,1024]{1,0:T(8,128)(2,1)S(1)} %collective-permute-done.5, f32[1024]{0:T(1024)S(1)} %bitcast.119, f32[1024]{0:T(1024)S(1)} %bitcast.120, f32[1024]{0:T(1024)S(1)} %bitcast.122, ...), kind=kLoop, calls=%fused_computation.88 | loop fusion | flops 47972352 | bytes 1236992 | tf_op jit(solution)/shard_map/convert_element_type | solution.py:148
  202.9 3.7 %convert_reduce_fusion = f32[32,1024]{1,0:T(8,128)} fusion(bf16[64,32,1024]{2,1,0:T(8,128)(2,1)} %all-to-all-done.2), kind=kLoop, calls=%fused_computation.2 | loop fusion | flops 4161536 | bytes 4325376 | tf_op jit(solution)/shard_map/reduce_sum | solution.py:126
  (67 shorter events, 3.0 us)
Async XLA Ops:
  0.6 77.7 %copy-start = (bf16[1,2048,512]{2,1,0:T(8,128)(2,1)S(1)}, bf16[1,2048,512]{2,1,0:T(8,128)(2,1)}, u32[]{:S(2)}) copy-start(bf16[1,2048,512]{2,1,0:T(8,128)(2,1)} %param.19) | copy-start | bytes 6291460
  70.8 13.0 %copy-start.2 = (bf16[64,8,4096]{2,1,0:T(8,128)(2,1)}, bf16[64,8,4096]{2,1,0:T(8,128)(2,1)S(1)}, u32[]{:S(2)}) copy-start(bf16[64,8,4096]{2,1,0:T(8,128)(2,1)S(1)} %all_to_all.15) | copy-start | bytes 12582916
  70.8 7.2 %collective-permute-start = (bf16[512,4096]{1,0:T(8,128)(2,1)S(1)}, bf16[512,4096]{1,0:T(8,128)(2,1)S(1)}, u32[]{:S(2)}, u32[]{:S(2)}) collective-permute-start(bf16[512,4096]{1,0:T(8,128)(2,1)S(1)} %bitcast.104), channel_id=1, source_target_pairs={{0,1},{1,0},{2,3},{3,2},{4,5},{5,4},{6,7},{7,6},{8,9},{9,8},{10,11... | collective-permute-start | bytes 12582920 | tf_op jit(solution)/shard_map/ppermute | solution.py:24
  78.0 5.8 %copy-start.6 = (bf16[512,4096]{1,0:T(8,128)(2,1)}, bf16[512,4096]{1,0:T(8,128)(2,1)S(1)}, u32[]{:S(2)}) copy-start(bf16[512,4096]{1,0:T(8,128)(2,1)S(1)} %collective-permute-done) | copy-start | bytes 12582916
  78.4 2.4 %copy-start.4 = (bf16[1024,2048]{1,0:T(8,128)(2,1)}, bf16[1024,2048]{1,0:T(8,128)(2,1)S(1)}, u32[]{:S(2)}) copy-start(bf16[1024,2048]{1,0:T(8,128)(2,1)S(1)} %fusion) | copy-start | bytes 12582916
  78.4 3.1 %copy-start.3 = (bf16[1,2048,512]{2,1,0:T(8,128)(2,1)S(1)}, bf16[1,2048,512]{2,1,0:T(8,128)(2,1)}, u32[]{:S(2)}) copy-start(bf16[1,2048,512]{2,1,0:T(8,128)(2,1)} %param.20) | copy-start | bytes 6291460
  81.5 2.4 %copy-start.17 = (f32[1024,512]{1,0:T(8,128)}, f32[1024,512]{1,0:T(8,128)S(1)}, u32[]{:S(2)}) copy-start(f32[1024,512]{1,0:T(8,128)S(1)} %fusion.8) | copy-start | bytes 6291460
  81.5 2.4 %copy-start.15 = (bf16[1,512,2048]{2,1,0:T(8,128)(2,1)S(1)}, bf16[1,512,2048]{2,1,0:T(8,128)(2,1)}, u32[]{:S(2)}) copy-start(bf16[1,512,2048]{2,1,0:T(8,128)(2,1)} %param.21) | copy-start | bytes 6291460
  83.8 4.4 %copy-start.18 = (f32[1024,512]{1,0:T(8,128)}, f32[1024,512]{1,0:T(8,128)S(1)}, u32[]{:S(2)}) copy-start(f32[1024,512]{1,0:T(8,128)S(1)} %fusion.12) | copy-start | bytes 6291460
  88.2 7.0 %copy-start.9 = (bf16[1024,512]{1,0:T(8,128)(2,1)}, bf16[1024,512]{1,0:T(8,128)(2,1)S(1)}, u32[]{:S(2)}) copy-start(bf16[1024,512]{1,0:T(8,128)(2,1)S(1)} %get-tuple-element.9) | copy-start | bytes 3145732
  90.8 4.4 %collective-permute-start.1 = (bf16[512,2048]{1,0:T(8,128)(2,1)S(1)}, bf16[512,2048]{1,0:T(8,128)(2,1)S(1)}, u32[]{:S(2)}, u32[]{:S(2)}) collective-permute-start(bf16[512,2048]{1,0:T(8,128)(2,1)S(1)} %add_convert_fusion.1), channel_id=1, source_target_pairs={{0,1},{1,0},{2,3},{3,2},{4,5},{5,4},{6,7},{7,6},{8,9},{9,8},{10,11... | collective-permute-start | bytes 6291464 | tf_op jit(solution)/shard_map/ppermute | solution.py:24
  98.0 7.5 %copy-start.13 = (f32[31,1024]{1,0:T(8,128)S(1)}, f32[31,1024]{1,0:T(8,128)}, u32[]{:S(2)}) copy-start(f32[31,1024]{1,0:T(8,128)} %param.16) | copy-start | bytes 380932
  98.0 40.2 %copy-start.16 = (f32[1024]{0:T(1024)S(1)}, f32[1024]{0:T(1024)}, u32[]{:S(2)}) copy-start(f32[1024]{0:T(1024)} %param.17) | copy-start | bytes 12292
  98.0 36.4 %all-to-all-start.1 = ((bf16[64,8,2048]{2,1,0:T(8,128)(2,1)}), bf16[64,8,2048]{2,1,0:T(8,128)(2,1)S(1)}, u32[]{:S(2)}, u32[]{:S(2)}) async-start(bf16[64,8,2048]{2,1,0:T(8,128)(2,1)} %fusion.1), calls=%async_computation.1 | async-start | bytes 4194304 | tf_op jit(solution)/shard_map/all_to_all | solution.py:92
  105.3 30.8 %collective-permute-start.3 = (f32[2,256]{1,0:T(2,128)S(1)}, f32[2,256]{1,0:T(2,128)S(1)}, u32[]{:S(2)}, u32[]{:S(2)}) collective-permute-start(f32[2,256]{1,0:T(2,128)S(1)} %pad_maximum_fusion.8), channel_id=1, source_target_pairs={{0,1},{1,0},{2,3},{3,2},{4,5},{5,4},{6,7},{7,6},{8,9},{9,8},{10,11... | collective-permute-start | bytes 6152 | tf_op jit(solution)/shard_map/ppermute | solution.py:24
  134.4 3.8 %copy-start.7 = (bf16[256,1024]{1,0:T(8,128)(2,1)S(1)}, bf16[256,1024]{1,0:T(8,128)(2,1)}, u32[]{:S(2)}) copy-start(bf16[256,1024]{1,0:T(8,128)(2,1)} %param.15) | copy-start | bytes 1572868
  136.1 2.0 collective-permute-start.2
  138.2 3.6 %copy-start.11 = (bf16[128,2048]{1,0:T(8,128)(2,1)}, bf16[128,2048]{1,0:T(8,128)(2,1)S(1)}, u32[]{:S(2)}) copy-start(bf16[128,2048]{1,0:T(8,128)(2,1)S(1)} %get-tuple-element.12) | copy-start | bytes 1572868
  141.8 61.1 %all-to-all-start.2 = ((bf16[64,32,1024]{2,1,0:T(8,128)(2,1)}), bf16[64,32,1024]{2,1,0:T(8,128)(2,1)}, u32[]{:S(2)}, u32[]{:S(2)}) async-start(bf16[64,32,1024]{2,1,0:T(8,128)(2,1)} %bitcast.108), calls=%async_computation.2 | async-start | bytes 8388608 | tf_op jit(solution)/shard_map/all_to_all | solution.py:119
  147.8 8.1 %copy-start.8 = (bf16[256,1024]{1,0:T(8,128)(2,1)S(1)}, bf16[256,1024]{1,0:T(8,128)(2,1)}, u32[]{:S(2)}) copy-start(bf16[256,1024]{1,0:T(8,128)(2,1)} %param.15) | copy-start | bytes 1572868
  147.8 8.1 %copy-start.12 = (bf16[128,2048]{1,0:T(8,128)(2,1)S(1)}, bf16[128,2048]{1,0:T(8,128)(2,1)}, u32[]{:S(2)}) copy-start(bf16[128,2048]{1,0:T(8,128)(2,1)} %copy-done.11) | copy-start | bytes 1572868
  147.8 8.1 %copy-start.14 = (bf16[1024,2048]{1,0:T(8,128)(2,1)S(1)}, bf16[1024,2048]{1,0:T(8,128)(2,1)}, u32[]{:S(2)}) copy-start(bf16[1024,2048]{1,0:T(8,128)(2,1)} %param.18) | copy-start | bytes 12582916
  155.9 2.2 %copy-start.5 = (bf16[1024,2048]{1,0:T(8,128)(2,1)S(1)}, bf16[1024,2048]{1,0:T(8,128)(2,1)}, u32[]{:S(2)}) copy-start(bf16[1024,2048]{1,0:T(8,128)(2,1)} %copy-done.4) | copy-start | bytes 12582916
  156.0 2.5 %copy-start.10 = (bf16[1024,512]{1,0:T(8,128)(2,1)S(1)}, bf16[1024,512]{1,0:T(8,128)(2,1)}, u32[]{:S(2)}) copy-start(bf16[1024,512]{1,0:T(8,128)(2,1)} %copy-done.9) | copy-start | bytes 3145732
  157.7 5.1 %collective-permute-start.4 = (f32[2,256]{1,0:T(2,128)S(1)}, f32[2,256]{1,0:T(2,128)S(1)}, u32[]{:S(2)}, u32[]{:S(2)}) collective-permute-start(f32[2,256]{1,0:T(2,128)S(1)} %pad_maximum_fusion.9), channel_id=1, source_target_pairs={{0,1},{1,0},{2,3},{3,2},{4,5},{5,4},{6,7},{7,6},{8,9},{9,8},{10,11... | collective-permute-start | bytes 6152 | tf_op jit(solution)/shard_map/ppermute | solution.py:24
  163.2 34.3 %collective-permute-start.5 = (bf16[15,1024]{1,0:T(8,128)(2,1)S(1)}, bf16[15,1024]{1,0:T(8,128)(2,1)S(1)}, u32[]{:S(2)}, u32[]{:S(2)}) collective-permute-start(bf16[15,1024]{1,0:T(8,128)(2,1)S(1)} %get-tuple-element.13), channel_id=1, source_target_pairs={{2,0},{4,2},{6,4},{8,6},{10,8},{12,10},{14,12},{16,14},{18,16},{20... | collective-permute-start | bytes 92168 | tf_op jit(solution)/shard_map/ppermute | solution.py:142
  164.5 33.0 %collective-permute-start.6 = (bf16[15,1024]{1,0:T(8,128)(2,1)S(1)}, bf16[15,1024]{1,0:T(8,128)(2,1)S(1)}, u32[]{:S(2)}, u32[]{:S(2)}) collective-permute-start(bf16[15,1024]{1,0:T(8,128)(2,1)S(1)} %get-tuple-element.14), channel_id=1, source_target_pairs={{0,2},{2,4},{4,6},{6,8},{8,10},{10,12},{12,14},{14,16},{16,18},{18... | collective-permute-start | bytes 92168 | tf_op jit(solution)/shard_map/ppermute | solution.py:139
  169.1 37.5 %copy-start.1 = (bf16[1,2048,512]{2,1,0:T(8,128)(2,1)S(1)}, bf16[1,2048,512]{2,1,0:T(8,128)(2,1)}, u32[]{:S(2)}) copy-start(bf16[1,2048,512]{2,1,0:T(8,128)(2,1)} %param.19) | copy-start | bytes 6291460
